TPU v7x, 256 devices: a whole 4x4x8 slice. The times are simulated.
256 devices in a mesh: sp: 64 (over z, x, core), tp: 4 (over y).
Axes of the slice: x: 4, y: 4, z: 8, core: 2. Of those that a mesh axis runs over, the one named last changes fastest.
Arguments:
- stream: bfloat16 [32768, 2048], P(('sp', 'tp')), may hold values from -6 to 6
- pool_in: bfloat16 [32768, 1024], P('sp', 'tp'), may hold values from -6 to 6
- doc_ids: int32 [32768], P('sp'), may hold values from 0 to 7, never falling along the last dimension, each value on 1 to 8192 neighbouring positions
- pool_map: bfloat16 [4, 256, 512], P('tp'), may hold values from -0.375 to 0.375
- pool_scale: float32 [2048], P('tp'), may hold values from 0.1 to 1.9
- out_weight: bfloat16 [2048, 2048], P('tp'), may hold values from -0.125 to 0.125
- norm_gain: float32 [2048], replicated, may hold values from 0.1 to 1.9
- routes: int32 [32768, 2], P('sp'), may hold values from 0 to 63, all different within a row; in each aligned block of 128 rows (0 to 127, 128 to 255, ...) at most 6 rows name the same one
- route_weight: float32 [32768, 2], P(('sp', 'tp')), may hold values from 0.2 to 1
- expert_gate: bfloat16 [64, 2048, 1024], P('sp', None, 'tp'), may hold values from -0.125 to 0.125
- expert_up: bfloat16 [64, 2048, 1024], P('sp', None, 'tp'), may hold values from -0.125 to 0.125
- expert_down: bfloat16 [64, 1024, 2048], P('sp', 'tp'), may hold values from -0.1875 to 0.1875
Outputs:
- result: bfloat16 [32768, 2048], P(('sp', 'tp'))
Inputs may be any that keep to these rules, and one draw needn't show every extreme that they name: `routes`: each token names 2 different experts; in each aligned block of 128 rows no expert is named by more than 6 rows, a bound that some block reaches. `doc_ids`: never falling; each document holds at most 8192 positions.
All inputs are finite; a program needn't handle non-finite values.
Results may differ from a plain program's by a relative error of at most 0.014.
Values may be sent and summed in bfloat16 or wider, within the bound.
No kernel may reach another device: no remote copies, remote signals or barrier semaphores. Data moves between devices by JAX's collectives and lax.ppermute only.
A program may use at most 64 MiB of HBM per device.

v0:
```python
import jax
import jax.numpy as jnp
from jax import lax
from jax.sharding import PartitionSpec as P

SPAN = 16
EPS = 1e-06


def passed_along(value, axis, by):
    length = lax.axis_size(axis)
    pairs = [(i, i + by) for i in range(length) if 0 <= i + by < length]
    return lax.ppermute(value, axis, pairs)


def cut_along(value, dim, length):
    before, after = (value.shape[:dim], value.shape[dim + 1 :])
    return jnp.moveaxis(value.reshape(*before, length, -1, *after), dim, 0)


def sum_at_owner(value, axis, dim):
    length = lax.axis_size(axis)
    tiles = lax.all_to_all(cut_along(value, dim, length), axis, 0, 0, tiled=True)
    return jnp.sum(tiles.astype(jnp.float32), axis=0)


def slot_table(route_block, expert_count, capacity, top_count):
    flattened = route_block.reshape(-1)
    one_hot = (flattened[:, None] == jnp.arange(expert_count, dtype=jnp.int32)[None, :]).astype(
        jnp.int32
    )
    ranking = jnp.sum((jnp.cumsum(one_hot, axis=0) - one_hot) * one_hot, axis=1)
    target_slot = flattened * capacity + ranking
    matches = target_slot[None, :] == jnp.arange(expert_count * capacity, dtype=jnp.int32)[:, None]
    sources = jnp.sum(
        jnp.where(matches, jnp.arange(flattened.shape[0], dtype=jnp.int32)[None, :], 0), axis=1
    )
    filled = jnp.any(matches, axis=1)
    return (target_slot, sources // top_count, filled)


def per_device(
    stream,
    pool_in,
    doc_ids,
    pool_map,
    pool_scale,
    out_weight,
    norm_gain,
    routes,
    route_weight,
    expert_gate,
    expert_up,
    expert_down,
):
    row_count = pool_in.shape[0]
    model_width = stream.shape[1]
    top_count = routes.shape[1]
    tp_count = lax.axis_size("tp")
    expert_count = lax.axis_size("sp")
    quarter = row_count // tp_count
    capacity = max(2, 3 * top_count * quarter // (2 * expert_count))
    reach_rows = SPAN - 1
    tail_rows = (
        pool_in[row_count - reach_rows :],
        doc_ids[row_count - reach_rows :].astype(jnp.bfloat16),
    )
    prior_rows, prior_docs = passed_along((tail_rows[0], tail_rows[1]), "sp", 1)
    extended = jnp.concatenate([prior_rows, pool_in], axis=0).astype(jnp.float32)
    extended_docs = jnp.concatenate([prior_docs.astype(jnp.float32), doc_ids.astype(jnp.float32)])
    own_docs = doc_ids.astype(jnp.float32)
    window = jnp.left_shift(jnp.int32(2), lax.axis_index("tp"))
    positions = lax.axis_index("sp") * row_count + jnp.arange(row_count, dtype=jnp.int32)
    running = jnp.zeros(pool_in.shape, jnp.float32)
    counts = jnp.zeros((row_count,), jnp.float32)
    for offset in range(reach_rows + 1):
        begin_row = reach_rows - offset
        piece_rows = extended[begin_row : begin_row + row_count]
        piece_docs = extended_docs[begin_row : begin_row + row_count]
        in_window = (offset < window) & (positions - offset >= 0) & (piece_docs == own_docs)
        running = running + jnp.where(in_window[:, None], piece_rows, 0.0)
        counts = counts + in_window.astype(jnp.float32)
    pooled = (running / counts[:, None] - pool_in.astype(jnp.float32)).astype(jnp.bfloat16)
    branch = (jnp.dot(pooled, pool_map[0], preferred_element_type=jnp.float32) * pool_scale).astype(
        jnp.bfloat16
    )
    projected = sum_at_owner(
        jnp.dot(branch, out_weight, preferred_element_type=jnp.float32).astype(jnp.bfloat16),
        "tp",
        0,
    )
    mixed_rows = (stream.astype(jnp.float32) + projected).astype(jnp.bfloat16)
    mixed_up = mixed_rows.astype(jnp.float32)
    normed = (
        mixed_up * lax.rsqrt(jnp.mean(mixed_up * mixed_up, axis=1, keepdims=True) + EPS) * norm_gain
    ).astype(jnp.bfloat16)
    own_routes = lax.dynamic_slice_in_dim(routes, lax.axis_index("tp") * quarter, quarter, 0)
    own_slots, own_sources, own_filled = slot_table(own_routes, expert_count, capacity, top_count)
    token_index = own_sources.reshape(expert_count, 1, capacity)
    filled_slots = own_filled.reshape(expert_count, 1, capacity)
    dispatch = jnp.where(filled_slots[..., None], normed[token_index], jnp.zeros((), jnp.bfloat16))
    arrived = lax.all_to_all(dispatch, "sp", split_axis=0, concat_axis=0, tiled=True)
    arrived = lax.all_gather(arrived, "tp", axis=1, tiled=True)
    stacked = arrived.reshape(-1, model_width)
    gate_pre = jnp.dot(stacked, expert_gate[0], preferred_element_type=jnp.float32)
    up_pre = jnp.dot(stacked, expert_up[0], preferred_element_type=jnp.float32)
    hidden = (jax.nn.silu(gate_pre) * up_pre).astype(jnp.bfloat16)
    partial_out = jnp.dot(hidden, expert_down[0], preferred_element_type=jnp.float32).reshape(
        arrived.shape
    )
    summed = sum_at_owner(partial_out.astype(jnp.bfloat16), "tp", 1).astype(jnp.bfloat16)
    returned = lax.all_to_all(summed, "sp", split_axis=0, concat_axis=0, tiled=True)
    outputs = returned.reshape(expert_count * capacity, model_width)
    picked = outputs[own_slots].astype(jnp.float32).reshape(quarter, top_count, model_width)
    combined = jnp.sum(route_weight[:, :, None] * picked, axis=1)
    return (mixed_up + combined).astype(jnp.bfloat16)


def solution(mesh):
    in_specs = (
        P(("sp", "tp"), None),
        P("sp", "tp"),
        P("sp"),
        P("tp", None, None),
        P("tp"),
        P("tp", None),
        P(),
        P("sp", None),
        P(("sp", "tp"), None),
        P("sp", None, "tp"),
        P("sp", None, "tp"),
        P("sp", "tp", None),
    )
    out_specs = P(("sp", "tp"), None)
    return jax.shard_map(
        per_device, mesh=mesh, in_specs=in_specs, out_specs=out_specs, check_vma=False
    )
```

profile of v0, /device:TPU:2, one launch (start us, length us, event | category | flops | bytes accessed | tf_op | source)
XLA Modules:
  0.0 378.5 jit_solution(2949899418363238842)
XLA Ops:
  6.5 0.0 copy-start
  6.5 0.9 fusion.128
  7.4 0.1 slice.108
  7.5 1.9 collective-permute-start.1
  9.4 0.7 slice.106
  10.1 3.5 collective-permute-start
  13.6 0.0 collective-permute-done.1
  13.6 0.1 pad_maximum_fusion
  13.7 0.8 convert_add_fusion.1
  14.5 0.5 collective-permute-done
  15.0 1.0 maximum_convert_fusion
  16.1 0.0 copy-done
  16.1 5.4 %convolution_convert_fusion = bf16[512,2048]{1,0:T(8,128)(2,1)} fusion(bf16[512,2048]{1,0:T(8,128)(2,1)S(1)} %copy-done, f32[512]{0:T(512)} %param.16, bf16[512,256]{1,0:T(8,128)(2,1)} %param.13, f32[527,256]{1,0:T(8,128)S(1)} %maximum_convert_fusion, bf16[1,256,512]{2,1,0:T(8,128)(2,1)} %param.15, f32[512]{0:T(512)S(1)} %get-tuple-element.9, ...), kind=kOutput, calls=%fused_computation.5 | convolution fusion | flops 1214119936 | bytes 13119488 | tf_op jit(solution)/shard_map/dot_general | solution.py:88
  21.5 4.5 %all-to-all-start = ((bf16[4,128,2048]{2,1,0:T(8,128)(2,1)}), bf16[4,128,2048]{2,1,0:T(8,128)(2,1)S(1)}, u32[]{:S(2)}, u32[]{:S(2)}) async-start(bf16[4,128,2048]{2,1,0:T(8,128)(2,1)} %bitcast.58), calls=%async_computation | async-start | bytes 4194304 | tf_op jit(solution)/shard_map/all_to_all | solution.py:23
  25.9 0.0 all-gather.2.cloned.1.call-start
  25.9 0.7 broadcast_multiply_fusion
  26.7 0.1 copy.35
  26.8 0.1 eq.103
  26.9 0.1 reshape.209
  27.1 0.6 reduce-window.6
  27.7 0.2 slice_reduce_fusion
  27.9 0.1 fusion.73
  28.0 0.2 select_reduce_fusion
  28.2 0.1 reduce_sum.67
  28.4 0.1 reshape.217
  28.5 0.2 fusion.30
  28.7 0.2 broadcast_in_dim.172
  28.8 0.0 copy-start.5
  28.9 23.3 %all-to-all-done = bf16[4,128,2048]{2,1,0:T(8,128)(2,1)S(1)} async-done(((bf16[4,128,2048]{2,1,0:T(8,128)(2,1)}), bf16[4,128,2048]{2,1,0:T(8,128)(2,1)S(1)}, u32[]{:S(2)}, u32[]{:S(2)}) %all-to-all-start) | async-done | bytes 2097184 | tf_op jit(solution)/shard_map/all_to_all | solution.py:23
  52.1 0.4 convert_reduce_fusion
  52.5 0.0 copy-done.4
  52.5 0.3 fusion.2
  52.8 0.2 fusion.4
  53.0 2.5 gather_fusion
  55.4 1.6 reshape.216
  57.1 1.8 select_bitcast_fusion
  58.9 62.8 %all_to_all.20 = bf16[64,1,6,2048]{3,2,1,0:T(8,128)(2,1)S(1)} all-to-all(bf16[64,1,6,2048]{3,2,1,0:T(8,128)(2,1)S(1)} %select_bitcast_fusion), channel_id=1, replica_groups=mesh['sp'=64,'tp'=4] {'sp'}, dimensions={0} | all-to-all | bytes 3145728 | tf_op jit(solution)/shard_map/all_to_all | solution.py:102
  121.7 2.0 copy.39
  123.7 0.0 all-gather.2.cloned.1.call-update
  123.7 62.7 %all-gather.2.cloned.1.call-done = bf16[64,4,6,2048]{3,0,2,1:T(8,128)(2,1)} async-done(((bf16[64,1,6,2048]{3,0,2,1:T(8,128)(2,1)}), bf16[64,4,6,2048]{3,0,2,1:T(8,128)(2,1)}) %all-gather.2.cloned.1.call-update) | async-done | bytes 6291472 | tf_op jit(solution)/shard_map/all_gather | solution.py:103
  186.4 9.6 %copy.40 = bf16[64,4,6,2048]{3,2,1,0:T(8,128)(2,1)} copy(bf16[64,4,6,2048]{3,0,2,1:T(8,128)(2,1)} %all-gather.2.cloned.1.call-done) | data formatting | bytes 12582912 | tf_op jit(solution)/shard_map/all_gather | solution.py:103
  196.0 11.1 %reshape.211 = bf16[1536,2048]{1,0:T(8,128)(2,1)} reshape(bf16[64,4,6,2048]{3,2,1,0:T(8,128)(2,1)} %copy.40) | data formatting | bytes 12582912 | tf_op jit(solution)/shard_map/reshape | solution.py:104
  207.2 4.8 %fusion.8 = f32[1536,256]{1,0:T(8,128)S(1)} fusion(bf16[1536,2048]{1,0:T(8,128)(2,1)} %reshape.211, bf16[1,2048,256]{2,1,0:T(8,128)(2,1)S(1)} %copy-done.7), kind=kOutput, calls=%fused_computation.21 | convolution fusion | flops 1610612736 | bytes 8912896 | tf_op jit(solution)/shard_map/dot_general | solution.py:105
  212.0 0.0 copy-done.2
  212.0 0.0 copy-done.8
  212.0 2.1 fusion
  214.1 0.0 copy-start.3
  214.1 0.3 dot_general.21
  214.4 0.9 copy-done.3
  215.3 2.0 convert_bitcast_fusion
  217.4 74.6 %all_to_all.21 = bf16[4,64,1,6,2048]{4,1,3,2,0:T(8,128)(2,1)S(1)} all-to-all(bf16[4,64,1,6,2048]{4,1,3,2,0:T(8,128)(2,1)S(1)} %convert_bitcast_fusion), channel_id=1, replica_groups=mesh['sp'=64,'tp'=4] {'tp'}, dimensions={0} | all-to-all | bytes 12582912 | tf_op jit(solution)/shard_map/all_to_all | solution.py:23
  291.9 1.2 bitcast_reduce_fusion
  293.2 2.2 copy.44
  295.4 10.9 %all-to-all-start.3 = ((bf16[64,1,6,2048]{3,2,1,0:T(8,128)(2,1)}), bf16[64,1,6,2048]{3,2,1,0:T(8,128)(2,1)}, u32[]{:S(2)}, u32[]{:S(2)}) async-start(bf16[64,1,6,2048]{3,2,1,0:T(8,128)(2,1)} %copy.44), calls=%async_computation.3 | async-start | bytes 4194304 | tf_op jit(solution)/shard_map/all_to_all | solution.py:112
  306.2 0.1 copy.45
  306.3 0.1 mul.92
  306.5 0.0 copy-done.6
  306.5 0.1 copy.34
  306.6 50.8 %all-to-all-done.3 = bf16[64,1,6,2048]{3,2,1,0:T(8,128)(2,1)} async-done(((bf16[64,1,6,2048]{3,2,1,0:T(8,128)(2,1)}), bf16[64,1,6,2048]{3,2,1,0:T(8,128)(2,1)}, u32[]{:S(2)}, u32[]{:S(2)}) %all-to-all-start.3) | async-done | bytes 1572896 | tf_op jit(solution)/shard_map/all_to_all | solution.py:112
  357.4 2.6 reshape.213
  360.0 2.3 gather_fusion.1
  362.3 3.5 reshape.214
  365.9 4.8 %multiply_reduce_fusion = f32[128,2048]{1,0:T(8,128)S(1)} fusion(f32[128,2,2048]{2,1,0:T(2,128)} %reshape.214, f32[128,2]{1,0:T(8,128)S(1)} %copy.34), kind=kLoop, calls=%fused_computation.8 | loop fusion | flops 786432 | bytes 3146752 | tf_op jit(solution)/shard_map/reduce_sum | solution.py:115
  370.7 0.9 fusion.5
  (19 shorter events, 0.1 us)
Async XLA Ops:
  6.5 9.5 %copy-start = (bf16[512,2048]{1,0:T(8,128)(2,1)S(1)}, bf16[512,2048]{1,0:T(8,128)(2,1)}, u32[]{:S(2)}) copy-start(bf16[512,2048]{1,0:T(8,128)(2,1)} %param.17) | copy-start | bytes 6291460
  7.5 6.2 %collective-permute-start.1 = (bf16[15]{0:T(256)(128)(2,1)S(1)}, bf16[15]{0:T(256)(128)(2,1)S(1)}, u32[]{:S(2)}, u32[]{:S(2)}) collective-permute-start(bf16[15]{0:T(256)(128)(2,1)S(1)} %slice.108), channel_id=1, source_target_pairs={{0,4},{4,8},{8,12},{12,16},{16,20},{20,24},{24,28},{28,32},{32,36}... | collective-permute-start | bytes 98 | tf_op jit(solution)/shard_map/ppermute | solution.py:13
  10.1 5.0 %collective-permute-start = (bf16[15,256]{1,0:T(8,128)(2,1)S(1)}, bf16[15,256]{1,0:T(8,128)(2,1)S(1)}, u32[]{:S(2)}, u32[]{:S(2)}) collective-permute-start(bf16[15,256]{1,0:T(8,128)(2,1)S(1)} %slice.106), channel_id=1, source_target_pairs={{0,4},{4,8},{8,12},{12,16},{16,20},{20,24},{24,28},{28,32},{32,36}... | collective-permute-start | bytes 23048 | tf_op jit(solution)/shard_map/ppermute | solution.py:13
  21.5 30.6 %all-to-all-start = ((bf16[4,128,2048]{2,1,0:T(8,128)(2,1)}), bf16[4,128,2048]{2,1,0:T(8,128)(2,1)S(1)}, u32[]{:S(2)}, u32[]{:S(2)}) async-start(bf16[4,128,2048]{2,1,0:T(8,128)(2,1)} %bitcast.58), calls=%async_computation | async-start | bytes 4194304 | tf_op jit(solution)/shard_map/all_to_all | solution.py:23
  25.9 26.6 %copy-start.4 = (bf16[128,2048]{1,0:T(8,128)(2,1)S(1)}, bf16[128,2048]{1,0:T(8,128)(2,1)}, u32[]{:S(2)}) copy-start(bf16[128,2048]{1,0:T(8,128)(2,1)} %param.12) | copy-start | bytes 1572868
  25.9 160.5 %all-gather.2.cloned.1.call-start = ((), (), s32[]{:S(2)}) async-start(), calls=%async_computation.4 | async-start | bytes 7864320 | tf_op jit(solution)/shard_map/all_gather | solution.py:103
  28.8 23.9 %copy-start.5 = (f32[2048]{0:T(1024)S(1)}, f32[2048]{0:T(1024)}, u32[]{:S(2)}) copy-start(f32[2048]{0:T(1024)} %param.18) | copy-start | bytes 24580
  196.0 11.1 %copy-start.7 = (bf16[1,2048,256]{2,1,0:T(8,128)(2,1)S(1)}, bf16[1,2048,256]{2,1,0:T(8,128)(2,1)}, u32[]{:S(2)}) copy-start(bf16[1,2048,256]{2,1,0:T(8,128)(2,1)} %param.21) | copy-start | bytes 3145732
  207.2 4.8 %copy-start.2 = (bf16[1536,2048]{1,0:T(8,128)(2,1)S(1)}, bf16[1536,2048]{1,0:T(8,128)(2,1)}, u32[]{:S(2)}) copy-start(bf16[1536,2048]{1,0:T(8,128)(2,1)} %reshape.211) | copy-start | bytes 18874372
  207.2 4.9 %copy-start.8 = (bf16[1,2048,256]{2,1,0:T(8,128)(2,1)S(1)}, bf16[1,2048,256]{2,1,0:T(8,128)(2,1)}, u32[]{:S(2)}) copy-start(bf16[1,2048,256]{2,1,0:T(8,128)(2,1)} %param.22) | copy-start | bytes 3145732
  214.1 1.2 copy-start.3
  295.4 11.1 %copy-start.6 = (f32[128,2]{0,1:T(2,128)S(1)}, f32[128,2]{0,1:T(2,128)}, u32[]{:S(2)}) copy-start(f32[128,2]{0,1:T(2,128)} %param.20) | copy-start | bytes 3076
  295.4 62.0 %all-to-all-start.3 = ((bf16[64,1,6,2048]{3,2,1,0:T(8,128)(2,1)}), bf16[64,1,6,2048]{3,2,1,0:T(8,128)(2,1)}, u32[]{:S(2)}, u32[]{:S(2)}) async-start(bf16[64,1,6,2048]{3,2,1,0:T(8,128)(2,1)} %copy.44), calls=%async_computation.3 | async-start | bytes 4194304 | tf_op jit(solution)/shard_map/all_to_all | solution.py:112
  362.3 9.3 %copy-start.1 = (bf16[512,2048]{1,0:T(8,128)(2,1)S(1)}, bf16[512,2048]{1,0:T(8,128)(2,1)}, u32[]{:S(2)}) copy-start(bf16[512,2048]{1,0:T(8,128)(2,1)} %param.17) | copy-start | bytes 6291460
Sparse Core Ops, SparseCore 0:
  123.8 62.5 all-gather.1
where the time goes:
time: 379 us; the launch traced here: 378 us
  waiting for transfers between devices  137 us (36%)
  blocking collectives  137 us (36%)
  local copies, waits for them, and re-layouts  40.9 us (11%)
  starting transfers between devices  20.7 us (5%)
  matrix products  14.3 us (4%)
  other arithmetic  14.2 us (4%)
  between operations  13.7 us (4%)
    all_to_all x1, blocking collectives, sum_at_owner(): lax.all_to_all(cut_along(value, dim, length), axis, 0, 0, tiled=True)  74.6 us
    all_to_all x1, blocking collectives, per_device(): lax.all_to_all(dispatch, 'sp', split_axis=0, concat_axis=0, tiled=True)  62.8 us
    all_gather x1, waiting for transfers between devices, per_device(): arrived = lax.all_gather(arrived, 'tp', axis=1, tiled=True)  62.7 us
    all_to_all x1, waiting for transfers between devices, per_device(): lax.all_to_all(summed, 'sp', split_axis=0, concat_axis=0, tiled=True)  50.8 us
    all_to_all x1, waiting for transfers between devices, sum_at_owner(): lax.all_to_all(cut_along(value, dim, length), axis, 0, 0, tiled=True)  23.3 us
    reshape x1, local copies, waits for them, and re-layouts, per_device(): stacked = arrived.reshape(-1, model_width)  11.1 us
    all_to_all x1, starting transfers between devices, per_device(): lax.all_to_all(summed, 'sp', split_axis=0, concat_axis=0, tiled=True)  10.9 us
    all_gather x1, local copies, waits for them, and re-layouts, per_device(): arrived = lax.all_gather(arrived, 'tp', axis=1, tiled=True)  9.61 us
  transfers between devices with their start and end apart: 5, of which 4 were waited for; matrix products, arithmetic and copies ran while one was open for 1% of the time, Pallas kernels for 0%

commit v1 on v0

--- a/solution.py
+++ b/solution.py
@@ -2,6 +2,7 @@
 import jax.numpy as jnp
 from jax import lax
 from jax.sharding import PartitionSpec as P
+from jax.lax import axis_index, axis_size, ppermute
 
 SPAN = 16
 EPS = 1e-06
@@ -100,7 +101,22 @@
     filled_slots = own_filled.reshape(expert_count, 1, capacity)
     dispatch = jnp.where(filled_slots[..., None], normed[token_index], jnp.zeros((), jnp.bfloat16))
     arrived = lax.all_to_all(dispatch, "sp", split_axis=0, concat_axis=0, tiled=True)
-    arrived = lax.all_gather(arrived, "tp", axis=1, tiled=True)
+    mixed_arr = axis_size("tp")
+    f_next = axis_index("tp")
+    o_now, small, r_now = (mixed_arr, f_next, arrived.shape[1])
+    panels = [(h, (h + 1) % o_now) for h in range(o_now)]
+    sheets = [(h, (h - 1) % o_now) for h in range(o_now)]
+    z2 = jnp.zeros((*arrived.shape[:1], o_now * r_now, *arrived.shape[2:]), arrived.dtype)
+    z2 = lax.dynamic_update_slice_in_dim(z2, arrived, small * r_now, axis=1)
+    far_arr = then = arrived
+    local_part = o_now // 2
+    for c in range(1, local_part + 1):
+        far_arr = ppermute(far_arr, "tp", panels)
+        z2 = lax.dynamic_update_slice_in_dim(z2, far_arr, (small - c) % o_now * r_now, axis=1)
+        if c < o_now - local_part:
+            then = ppermute(then, "tp", sheets)
+            z2 = lax.dynamic_update_slice_in_dim(z2, then, (small + c) % o_now * r_now, axis=1)
+    arrived = z2
     stacked = arrived.reshape(-1, model_width)
     gate_pre = jnp.dot(stacked, expert_gate[0], preferred_element_type=jnp.float32)
     up_pre = jnp.dot(stacked, expert_up[0], preferred_element_type=jnp.float32)

time: 379 us -> 367 us (0.968)
  between operations: 13.7 us -> 0.31 us
  local copies, waits for them, and re-layouts: 40.9 us -> 48 us
  waiting for transfers between devices: 137 us -> 130 us
  starting transfers between devices: 20.7 us -> 25.4 us
    all_gather x1 -> x0, waiting for transfers between devices: 62.7 us -> none  [per_device(): arrived = lax.all_gather(arrived, 'tp', axis=1, tiled=True)]
    ppermute x0 -> x3, waiting for transfers between devices: none -> 55.2 us  [the longest x2 55.2 us: per_device(): far_arr = ppermute(far_arr, 'tp', panels)]
    dynamic_update_slice x0 -> x4, local copies, waits for them, and re-layouts: none -> 12.3 us  [the longest x2 7.2 us: per_device(): lax.dynamic_update_slice_in_dim(z2, far_arr, (small - c) % o_now * r_now,...]
    all_gather x1 -> x0, local copies, waits for them, and re-layouts: 9.61 us -> none  [per_device(): arrived = lax.all_gather(arrived, 'tp', axis=1, tiled=True)]
    broadcast_in_dim x0 -> x1, local copies, waits for them, and re-layouts: none -> 4.29 us  [per_device(): jnp.zeros((*arrived.shape[:1], o_now * r_now, *arrived.shape[2:]), arrive...]
  transfers between devices with their start and end apart: 5 -> 7, of which waited for: 4 -> 5; matrix products, arithmetic and copies ran while one was open for 1% -> 5% of each run, Pallas kernels for 0% -> 0%
where the time goes in v1:
time: 367 us; the launch traced here: 366 us
  blocking collectives  134 us (37%)
  waiting for transfers between devices  130 us (35%)
  local copies, waits for them, and re-layouts  48 us (13%)
  starting transfers between devices  25.4 us (7%)
  matrix products  14.3 us (4%)
  other arithmetic  14.2 us (4%)
    all_to_all x1, blocking collectives, sum_at_owner(): lax.all_to_all(cut_along(value, dim, length), axis, 0, 0, tiled=True)  71 us
    all_to_all x1, blocking collectives, per_device(): lax.all_to_all(dispatch, 'sp', split_axis=0, concat_axis=0, tiled=True)  62.8 us
    ppermute x2, waiting for transfers between devices, per_device(): far_arr = ppermute(far_arr, 'tp', panels)  55.2 us
    all_to_all x1, waiting for transfers between devices, per_device(): lax.all_to_all(summed, 'sp', split_axis=0, concat_axis=0, tiled=True)  50.8 us
    all_to_all x1, waiting for transfers between devices, sum_at_owner(): lax.all_to_all(cut_along(value, dim, length), axis, 0, 0, tiled=True)  23.3 us
    all_to_all x1, starting transfers between devices, per_device(): lax.all_to_all(summed, 'sp', split_axis=0, concat_axis=0, tiled=True)  12.3 us
    reshape x1, local copies, waits for them, and re-layouts, per_device(): stacked = arrived.reshape(-1, model_width)  11.1 us
  transfers between devices with their start and end apart: 7, of which 5 were waited for; matrix products, arithmetic and copies ran while one was open for 5% of the time, Pallas kernels for 0%

profile of v1, /device:TPU:2, one launch (start us, length us, event | category | flops | bytes accessed | tf_op | source)
XLA Modules:
  0.0 365.7 jit_solution(7192263257635174421)
XLA Ops:
  0.0 0.9 fusion.130
  0.9 0.1 slice.108
  0.9 1.9 collective-permute-start.1
  2.8 0.7 slice.106
  3.6 3.5 collective-permute-start
  7.1 0.1 pad_maximum_fusion
  7.2 0.8 convert_add_fusion.1
  8.0 0.5 collective-permute-done
  8.5 1.0 maximum_convert_fusion
  9.5 5.4 %convolution_convert_fusion = bf16[512,2048]{1,0:T(8,128)(2,1)} fusion(bf16[512,2048]{1,0:T(8,128)(2,1)S(1)} %copy-done, f32[512]{0:T(512)} %param.16, bf16[512,256]{1,0:T(8,128)(2,1)} %param.13, f32[527,256]{1,0:T(8,128)S(1)} %maximum_convert_fusion, bf16[1,256,512]{2,1,0:T(8,128)(2,1)} %param.15, f32[512]{0:T(512)S(1)} %get-tuple-element.9, ...), kind=kOutput, calls=%fused_computation.5 | convolution fusion | flops 1214119936 | bytes 13119488 | tf_op jit(solution)/shard_map/dot_general | solution.py:89
  14.9 4.5 %all-to-all-start = ((bf16[4,128,2048]{2,1,0:T(8,128)(2,1)}), bf16[4,128,2048]{2,1,0:T(8,128)(2,1)S(1)}, u32[]{:S(2)}, u32[]{:S(2)}) async-start(bf16[4,128,2048]{2,1,0:T(8,128)(2,1)} %bitcast.60), calls=%async_computation | async-start | bytes 4194304 | tf_op jit(solution)/shard_map/all_to_all | solution.py:24
  19.4 0.7 broadcast_multiply_fusion
  20.1 0.1 copy.41
  20.3 0.1 eq.107
  20.4 0.1 reshape.209
  20.5 0.6 reduce-window.6
  21.2 0.2 slice_reduce_fusion
  21.4 0.1 fusion.75
  21.5 0.2 select_reduce_fusion
  21.7 0.1 reduce_sum.67
  21.8 0.1 reshape.217
  22.0 0.2 fusion.32
  22.1 0.2 broadcast_in_dim.176
  22.3 0.0 copy-start.5
  22.3 23.3 %all-to-all-done = bf16[4,128,2048]{2,1,0:T(8,128)(2,1)S(1)} async-done(((bf16[4,128,2048]{2,1,0:T(8,128)(2,1)}), bf16[4,128,2048]{2,1,0:T(8,128)(2,1)S(1)}, u32[]{:S(2)}, u32[]{:S(2)}) %all-to-all-start) | async-done | bytes 2097184 | tf_op jit(solution)/shard_map/all_to_all | solution.py:24
  45.6 0.4 convert_reduce_fusion
  46.0 0.3 fusion.1
  46.2 0.2 fusion.3
  46.4 2.5 gather_fusion
  48.9 1.6 reshape.216
  50.5 1.8 select_bitcast_fusion
  52.4 62.8 %all_to_all.20 = bf16[64,1,6,2048]{3,2,1,0:T(8,128)(2,1)S(1)} all-to-all(bf16[64,1,6,2048]{3,2,1,0:T(8,128)(2,1)S(1)} %select_bitcast_fusion), channel_id=1, replica_groups=mesh['sp'=64,'tp'=4] {'sp'}, dimensions={0} | all-to-all | bytes 3145728 | tf_op jit(solution)/shard_map/all_to_all | solution.py:103
  115.1 2.0 copy.45
  117.2 0.6 collective-permute-start.2
  117.8 2.7 collective-permute-start.3
  120.4 32.9 %collective-permute-done.2 = bf16[64,1,6,2048]{3,0,2,1:T(8,128)(2,1)} collective-permute-done((bf16[64,1,6,2048]{3,0,2,1:T(8,128)(2,1)}, bf16[64,1,6,2048]{3,0,2,1:T(8,128)(2,1)}, u32[]{:S(2)}, u32[]{:S(2)}) %collective-permute-start.2) | collective-permute-done | bytes 1572896 | tf_op jit(solution)/shard_map/ppermute | solution.py:114
  153.3 0.0 collective-permute-start.4
  153.3 4.3 %broadcast_in_dim.175 = bf16[64,4,6,2048]{3,2,1,0:T(8,128)(2,1)} broadcast(bf16[]{:T(256)} %constant.139.clone.1), dimensions={} | broadcast | bytes 6291458 | tf_op jit(solution)/shard_map/broadcast_in_dim | solution.py:109
  157.6 1.5 constant_dynamic-update-slice_fusion
  159.2 3.6 copy_dynamic-update-slice_fusion.2
  162.7 3.6 copy_dynamic-update-slice_fusion.1
  166.3 22.3 %collective-permute-done.4 = bf16[64,1,6,2048]{3,0,2,1:T(8,128)(2,1)} collective-permute-done((bf16[64,1,6,2048]{3,0,2,1:T(8,128)(2,1)}, bf16[64,1,6,2048]{3,0,2,1:T(8,128)(2,1)}, u32[]{:S(2)}, u32[]{:S(2)}) %collective-permute-start.4) | collective-permute-done | bytes 1572896 | tf_op jit(solution)/shard_map/ppermute | solution.py:114
  188.6 3.6 copy_dynamic-update-slice_fusion
  192.3 11.1 %reshape.211 = bf16[1536,2048]{1,0:T(8,128)(2,1)} reshape(bf16[64,4,6,2048]{3,2,1,0:T(8,128)(2,1)} %copy_dynamic-update-slice_fusion) | data formatting | bytes 12582912 | tf_op jit(solution)/shard_map/reshape | solution.py:120
  203.4 4.8 %fusion.10 = f32[1536,256]{1,0:T(8,128)S(1)} fusion(bf16[1536,2048]{1,0:T(8,128)(2,1)} %reshape.211, bf16[1,2048,256]{2,1,0:T(8,128)(2,1)S(1)} %copy-done.7), kind=kOutput, calls=%fused_computation.24 | convolution fusion | flops 1610612736 | bytes 8912896 | tf_op jit(solution)/shard_map/dot_general | solution.py:121
  208.2 0.0 copy-done.8
  208.3 2.1 multiply_convert_fusion
  210.3 0.0 copy-start.3
  210.4 0.3 dot_general.21
  210.6 0.9 copy-done.3
  211.6 2.0 convert_bitcast_fusion
  213.6 71.0 %all_to_all.21 = bf16[4,64,1,6,2048]{4,1,3,2,0:T(8,128)(2,1)S(1)} all-to-all(bf16[4,64,1,6,2048]{4,1,3,2,0:T(8,128)(2,1)S(1)} %convert_bitcast_fusion), channel_id=1, replica_groups=mesh['sp'=64,'tp'=4] {'tp'}, dimensions={0} | all-to-all | bytes 12582912 | tf_op jit(solution)/shard_map/all_to_all | solution.py:24
  284.6 1.2 bitcast_reduce_fusion
  285.8 2.2 copy.53
  288.0 12.3 %all-to-all-start.3 = ((bf16[64,1,6,2048]{3,2,1,0:T(8,128)(2,1)}), bf16[64,1,6,2048]{3,2,1,0:T(8,128)(2,1)}, u32[]{:S(2)}, u32[]{:S(2)}) async-start(bf16[64,1,6,2048]{3,2,1,0:T(8,128)(2,1)} %copy.53), calls=%async_computation.3 | async-start | bytes 4194304 | tf_op jit(solution)/shard_map/all_to_all | solution.py:128
  300.3 0.1 copy.54
  300.4 0.1 mul.92
  300.6 0.1 copy.40
  300.7 50.8 %all-to-all-done.3 = bf16[64,1,6,2048]{3,2,1,0:T(8,128)(2,1)} async-done(((bf16[64,1,6,2048]{3,2,1,0:T(8,128)(2,1)}), bf16[64,1,6,2048]{3,2,1,0:T(8,128)(2,1)}, u32[]{:S(2)}, u32[]{:S(2)}) %all-to-all-start.3) | async-done | bytes 1572896 | tf_op jit(solution)/shard_map/all_to_all | solution.py:128
  351.5 2.6 reshape.213
  354.1 2.3 gather_fusion.1
  356.4 3.5 reshape.214
  360.0 4.8 %multiply_reduce_fusion = f32[128,2048]{1,0:T(8,128)S(1)} fusion(f32[128,2,2048]{2,1,0:T(2,128)} %reshape.214, f32[128,2]{1,0:T(8,128)S(1)} %copy.40), kind=kLoop, calls=%fused_computation.9 | loop fusion | flops 786432 | bytes 3146752 | tf_op jit(solution)/shard_map/reduce_sum | solution.py:131
  364.8 0.9 fusion.4
  (26 shorter events, 0.1 us)
Async XLA Ops:
  0.0 9.5 %copy-start = (bf16[512,2048]{1,0:T(8,128)(2,1)S(1)}, bf16[512,2048]{1,0:T(8,128)(2,1)}, u32[]{:S(2)}) copy-start(bf16[512,2048]{1,0:T(8,128)(2,1)} %param.17) | copy-start | bytes 6291460
  0.9 6.2 %collective-permute-start.1 = (bf16[15]{0:T(256)(128)(2,1)S(1)}, bf16[15]{0:T(256)(128)(2,1)S(1)}, u32[]{:S(2)}, u32[]{:S(2)}) collective-permute-start(bf16[15]{0:T(256)(128)(2,1)S(1)} %slice.108), channel_id=1, source_target_pairs={{0,4},{4,8},{8,12},{12,16},{16,20},{20,24},{24,28},{28,32},{32,36}... | collective-permute-start | bytes 98 | tf_op jit(solution)/shard_map/ppermute | solution.py:14
  3.6 5.0 %collective-permute-start = (bf16[15,256]{1,0:T(8,128)(2,1)S(1)}, bf16[15,256]{1,0:T(8,128)(2,1)S(1)}, u32[]{:S(2)}, u32[]{:S(2)}) collective-permute-start(bf16[15,256]{1,0:T(8,128)(2,1)S(1)} %slice.106), channel_id=1, source_target_pairs={{0,4},{4,8},{8,12},{12,16},{16,20},{20,24},{24,28},{28,32},{32,36}... | collective-permute-start | bytes 23048 | tf_op jit(solution)/shard_map/ppermute | solution.py:14
  14.9 30.6 %all-to-all-start = ((bf16[4,128,2048]{2,1,0:T(8,128)(2,1)}), bf16[4,128,2048]{2,1,0:T(8,128)(2,1)S(1)}, u32[]{:S(2)}, u32[]{:S(2)}) async-start(bf16[4,128,2048]{2,1,0:T(8,128)(2,1)} %bitcast.60), calls=%async_computation | async-start | bytes 4194304 | tf_op jit(solution)/shard_map/all_to_all | solution.py:24
  19.4 26.6 %copy-start.4 = (bf16[128,2048]{1,0:T(8,128)(2,1)S(1)}, bf16[128,2048]{1,0:T(8,128)(2,1)}, u32[]{:S(2)}) copy-start(bf16[128,2048]{1,0:T(8,128)(2,1)} %param.12) | copy-start | bytes 1572868
  22.3 23.9 %copy-start.5 = (f32[2048]{0:T(1024)S(1)}, f32[2048]{0:T(1024)}, u32[]{:S(2)}) copy-start(f32[2048]{0:T(1024)} %param.18) | copy-start | bytes 24580
  117.2 36.1 %collective-permute-start.2 = (bf16[64,1,6,2048]{3,0,2,1:T(8,128)(2,1)}, bf16[64,1,6,2048]{3,0,2,1:T(8,128)(2,1)}, u32[]{:S(2)}, u32[]{:S(2)}) collective-permute-start(bf16[64,1,6,2048]{3,0,2,1:T(8,128)(2,1)} %copy.45), channel_id=1, source_target_pairs={{0,1},{1,2},{2,3},{3,0},{4,5},{5,6},{6,7},{7,4},{8,9},{9,10},{10,1... | collective-permute-start | bytes 4718600 | tf_op jit(solution)/shard_map/ppermute | solution.py:114
  117.8 45.0 %collective-permute-start.3 = (bf16[64,1,6,2048]{3,0,2,1:T(8,128)(2,1)}, bf16[64,1,6,2048]{3,0,2,1:T(8,128)(2,1)}, u32[]{:S(2)}, u32[]{:S(2)}) collective-permute-start(bf16[64,1,6,2048]{3,0,2,1:T(8,128)(2,1)} %copy.45), channel_id=1, source_target_pairs={{0,3},{1,0},{2,1},{3,2},{4,7},{5,4},{6,5},{7,6},{8,11},{9,8},{10,9... | collective-permute-start | bytes 4718600 | tf_op jit(solution)/shard_map/ppermute | solution.py:117
  153.3 35.3 %collective-permute-start.4 = (bf16[64,1,6,2048]{3,0,2,1:T(8,128)(2,1)}, bf16[64,1,6,2048]{3,0,2,1:T(8,128)(2,1)}, u32[]{:S(2)}, u32[]{:S(2)}) collective-permute-start(bf16[64,1,6,2048]{3,0,2,1:T(8,128)(2,1)} %collective-permute-done.2), channel_id=1, source_target_pairs={{0,1},{1,2},{2,3},{3,0},{4,5},{5,6},{6,7},{7,4},{8,9},{9,10},{10,1... | collective-permute-start | bytes 4718600 | tf_op jit(solution)/shard_map/ppermute | solution.py:114
  192.3 11.1 %copy-start.7 = (bf16[1,2048,256]{2,1,0:T(8,128)(2,1)S(1)}, bf16[1,2048,256]{2,1,0:T(8,128)(2,1)}, u32[]{:S(2)}) copy-start(bf16[1,2048,256]{2,1,0:T(8,128)(2,1)} %param.21) | copy-start | bytes 3145732
  203.4 4.8 %copy-start.2 = (bf16[1536,2048]{1,0:T(8,128)(2,1)S(1)}, bf16[1536,2048]{1,0:T(8,128)(2,1)}, u32[]{:S(2)}) copy-start(bf16[1536,2048]{1,0:T(8,128)(2,1)} %reshape.211) | copy-start | bytes 18874372
  203.4 4.9 %copy-start.8 = (bf16[1,2048,256]{2,1,0:T(8,128)(2,1)S(1)}, bf16[1,2048,256]{2,1,0:T(8,128)(2,1)}, u32[]{:S(2)}) copy-start(bf16[1,2048,256]{2,1,0:T(8,128)(2,1)} %param.22) | copy-start | bytes 3145732
  210.3 1.2 copy-start.3
  288.0 12.6 %copy-start.6 = (f32[128,2]{0,1:T(2,128)S(1)}, f32[128,2]{0,1:T(2,128)}, u32[]{:S(2)}) copy-start(f32[128,2]{0,1:T(2,128)} %param.20) | copy-start | bytes 3076
  288.0 63.5 %all-to-all-start.3 = ((bf16[64,1,6,2048]{3,2,1,0:T(8,128)(2,1)}), bf16[64,1,6,2048]{3,2,1,0:T(8,128)(2,1)}, u32[]{:S(2)}, u32[]{:S(2)}) async-start(bf16[64,1,6,2048]{3,2,1,0:T(8,128)(2,1)} %copy.53), calls=%async_computation.3 | async-start | bytes 4194304 | tf_op jit(solution)/shard_map/all_to_all | solution.py:128
  356.4 9.3 %copy-start.1 = (bf16[512,2048]{1,0:T(8,128)(2,1)S(1)}, bf16[512,2048]{1,0:T(8,128)(2,1)}, u32[]{:S(2)}) copy-start(bf16[512,2048]{1,0:T(8,128)(2,1)} %param.17) | copy-start | bytes 6291460
